TPU v7x, 32 devices: a whole 2x2x4 slice. The times are simulated.
32 devices in a mesh: rep: 4 (over z), fs: 2 (over y), tp: 4 (over x, core).
Axes of the slice: x: 2, y: 2, z: 4, core: 2. Of those that a mesh axis runs over, the one named last changes fastest.
Arguments:
- inputs: bfloat16 [512, 4096], P('rep'), may hold values from -6 to 6
- cotangent: bfloat16 [512, 4096], P('rep'), may hold values from -6 to 6
- w_gate: bfloat16 [4096, 11264], P(None, ('fs', 'tp')), may hold values from -0.09375 to 0.09375
- w_upward: bfloat16 [4096, 11264], P(None, ('fs', 'tp')), may hold values from -0.09375 to 0.09375
- w_down: bfloat16 [11264, 4096], P(('fs', 'tp')), may hold values from -0.0546875 to 0.0546875
Outputs:
- grad_input: bfloat16 [512, 4096], P('rep')
- grad_gate: float32 [4096, 11264], P('rep', ('fs', 'tp'))
- grad_upward: float32 [4096, 11264], P('rep', ('fs', 'tp'))
- grad_down: float32 [11264, 4096], P(('fs', 'tp'), 'rep')
All inputs are finite; a program needn't handle non-finite values.
Results may differ from a plain program's by a relative error of at most 0.0049.
Values may be sent and summed in bfloat16 or wider, within the bound.
A program may use at most 128 MiB of HBM per device.

v0:
```python
import functools

import jax
import jax.numpy as jnp
from jax import lax
from jax.experimental import pallas as pl
from jax.experimental.pallas import tpu as pltpu
from jax.sharding import PartitionSpec as P

PLANE = ("fs", "tp")
MESH = pl.DeviceIdType.MESH


def contract_rows(left, right):
    return lax.dot_general(
        left, right, (((0,), (0,)), ((), ())), preferred_element_type=jnp.float32
    )


def contract_cols(left, right):
    return lax.dot_general(
        left, right, (((1,), (1,)), ((), ())), preferred_element_type=jnp.float32
    )


def greet(neighbours):
    barrier = pltpu.get_barrier_semaphore()
    for device in neighbours:
        pl.semaphore_signal(barrier, inc=1, device_id=device, device_id_type=MESH)
    pl.semaphore_wait(barrier, len(neighbours))


def gather_kernel(reps, x_ref, c_ref, all_x, all_c, send, recv, own_sem):
    z, y, t = lax.axis_index("rep"), lax.axis_index("fs"), lax.axis_index("tp")
    x, core = t // 2, t % 2
    half = (x + y) % 2
    mine = 2 * half + core
    across = 2 * (1 - half) + core
    up, down = (z + 1) % reps, (z + reps - 1) % reps
    to_up, to_down = (up, y, t), (down, y, t)
    x_near = (z, y, 2 * (x + 1 - 2 * (x % 2)) + core)
    y_near = (z, y + 1 - 2 * (y % 2), t)
    other = (z, y, 2 * x + 1 - core)
    greet((to_up, to_down, x_near, y_near, other))

    started = []

    def put(kind, step, src, dst, device):
        copy = pltpu.make_async_remote_copy(
            src_ref=src, dst_ref=dst, send_sem=send.at[kind, step],
            recv_sem=recv.at[kind, step], device_id=device, device_id_type=MESH,
        )
        copy.start()
        started.append(copy)
        return copy

    ring = [
        put(0, 0, x_ref.at[mine], all_x.at[z, mine], to_up),
        put(1, 0, c_ref.at[mine], all_c.at[z, mine], to_down),
    ]
    keep = [
        pltpu.make_async_copy(x_ref, all_x.at[z], own_sem.at[0]),
        pltpu.make_async_copy(c_ref, all_c.at[z], own_sem.at[1]),
    ]
    for copy in keep:
        copy.start()

    last = []

    def relay(sides, step, bx, bc):
        sides[0].wait_recv()
        last.append(put(6, step, all_x.at[bx, across], all_x.at[bx, across], other))
        sides[1].wait_recv()
        last.append(put(7, step, all_c.at[bc, across], all_c.at[bc, across], other))

    before = None
    for step in range(reps - 1):
        bx, bc = (z + reps - 1 - step) % reps, (z + 1 + step) % reps
        got_x, got_c = all_x.at[bx, mine], all_c.at[bc, mine]
        following = []
        ring[0].wait_recv()
        if step < reps - 2:
            following.append(put(0, step + 1, got_x, got_x, to_up))
        side_x = put(2, step, got_x, got_x, x_near)
        last.append(put(4, step, got_x, got_x, other))
        ring[1].wait_recv()
        if step < reps - 2:
            following.append(put(1, step + 1, got_c, got_c, to_down))
        side_c = put(3, step, got_c, got_c, y_near)
        last.append(put(5, step, got_c, got_c, other))
        if before is not None:
            relay(*before)
        before = ((side_x, side_c), step, bx, bc)
        ring = following
    relay(*before)
    for copy in last:
        copy.wait_recv()
    for copy in started:
        copy.wait_send()
    for copy in keep:
        copy.wait()


def gather(reps, inputs, cotangent):
    rows, width = inputs.shape
    quarter = (4, rows // 4, width)
    whole = jax.ShapeDtypeStruct((reps,) + quarter, inputs.dtype)
    vmem = pl.BlockSpec(memory_space=pltpu.VMEM)
    pair = pl.pallas_call(
        functools.partial(gather_kernel, reps),
        out_shape=(whole, whole),
        in_specs=[vmem, vmem],
        out_specs=(vmem, vmem),
        scratch_shapes=[
            pltpu.SemaphoreType.DMA((8, reps - 1)),
            pltpu.SemaphoreType.DMA((8, reps - 1)),
            pltpu.SemaphoreType.DMA((2,)),
        ],
        compiler_params=pltpu.CompilerParams(
            collective_id=0, has_side_effects=True, vmem_limit_bytes=60 * 2**20
        ),
        name="token_gather",
    )(inputs.reshape(quarter), cotangent.reshape(quarter))
    return [a.reshape(reps * rows, width) for a in pair]


def reduce_kernel(chips, across, terms, out, got, sums, landed, send, recv):
    z, y, t = lax.axis_index("rep"), lax.axis_index("fs"), lax.axis_index("tp")
    core = t % 2
    chip = y * across + t // 2
    other = (z, y, t + 1 - 2 * core)

    def peer(ahead):
        there = (chip + ahead) % chips
        return there, (z, there // across, 2 * (there % across) + core)

    greet([other] + [peer(ahead)[1] for ahead in range(1, chips)])

    def put(kind, slot, src, dst, device):
        copy = pltpu.make_async_remote_copy(
            src_ref=src, dst_ref=dst, send_sem=send.at[kind, slot],
            recv_sem=recv.at[kind, slot], device_id=device, device_id_type=MESH,
        )
        copy.start()
        return copy

    swaps = [put(0, j, terms.at[j, 1 - core], got.at[j], other) for j in range(chips)]
    for j in range(chips):
        swaps[j].wait_recv()
        pair = terms[j, core].astype(jnp.float32) + got[j].astype(jnp.float32)
        sums[j] = pair.astype(sums.dtype)
    spread = []
    for ahead in range(1, chips):
        there, device = peer(ahead)
        spread.append(put(1, ahead, sums.at[there], landed.at[ahead], device))
    total = terms[chip, core].astype(jnp.float32) + got[chip].astype(jnp.float32)
    for ahead in range(1, chips):
        spread[ahead - 1].wait_recv()
        total = total + landed[ahead].astype(jnp.float32)
    out[chip, core] = total.astype(out.dtype)
    done = out.at[chip, core]
    share = [put(2, ahead, done, done, peer(ahead)[1]) for ahead in range(1, chips)]
    relays = [put(3, 0, done, done, other)]
    for ahead in range(1, chips):
        share[ahead - 1].wait_recv()
        source = out.at[(chip + chips - ahead) % chips, core]
        relays.append(put(3, ahead, source, source, other))
    for copy in relays:
        copy.wait_recv()
    for copy in swaps + spread + share + relays:
        copy.wait_send()


def plane_sum(chips, across, terms):
    rows, width = terms.shape
    piece = (rows // (2 * chips), width)
    vmem = pl.BlockSpec(memory_space=pltpu.VMEM)
    total = pl.pallas_call(
        functools.partial(reduce_kernel, chips, across),
        out_shape=jax.ShapeDtypeStruct((chips, 2) + piece, terms.dtype),
        in_specs=[vmem],
        out_specs=vmem,
        scratch_shapes=[
            pltpu.VMEM((chips,) + piece, terms.dtype),
            pltpu.VMEM((chips,) + piece, terms.dtype),
            pltpu.VMEM((chips,) + piece, terms.dtype),
            pltpu.SemaphoreType.DMA((4, chips)),
            pltpu.SemaphoreType.DMA((4, chips)),
        ],
        compiler_params=pltpu.CompilerParams(
            collective_id=1, has_side_effects=True, vmem_limit_bytes=48 * 2**20
        ),
        name="plane_sum",
    )(terms.reshape((chips, 2) + piece))
    return total.reshape(rows, width)


def local(reps, chips, across, inputs, cotangent, w_gate, w_upward, w_down):
    rows, width = inputs.shape
    all_inputs, all_cotangent = gather(reps, inputs, cotangent)

    gate_pre = jnp.dot(all_inputs, w_gate, preferred_element_type=jnp.float32)
    up_pre = jnp.dot(all_inputs, w_upward, preferred_element_type=jnp.float32)
    sigmoid_gate = jax.nn.sigmoid(gate_pre)
    activated = gate_pre * sigmoid_gate
    hidden = (activated * up_pre).astype(jnp.bfloat16)
    hidden_grad = contract_cols(all_cotangent, w_down)
    gate_delta = (
        hidden_grad * up_pre * sigmoid_gate * (1.0 + gate_pre * (1.0 - sigmoid_gate))
    ).astype(jnp.bfloat16)
    up_delta = (hidden_grad * activated).astype(jnp.bfloat16)

    z = lax.axis_index("rep")
    own_gate = lax.dynamic_slice_in_dim(gate_delta, z * rows, rows, 0)
    own_up = lax.dynamic_slice_in_dim(up_delta, z * rows, rows, 0)
    terms = contract_cols(own_gate, w_gate) + contract_cols(own_up, w_upward)
    grad_input = plane_sum(chips, across, terms.astype(jnp.bfloat16))

    cols = width // reps
    input_cols = lax.dynamic_slice_in_dim(all_inputs, z * cols, cols, 1)
    cotangent_cols = lax.dynamic_slice_in_dim(all_cotangent, z * cols, cols, 1)
    grad_gate = contract_rows(input_cols, gate_delta)
    grad_upward = contract_rows(input_cols, up_delta)
    grad_down = contract_rows(hidden, cotangent_cols)
    return (grad_input, grad_gate, grad_upward, grad_down)


def solution(mesh):
    across = mesh.shape["tp"] // 2
    chips = mesh.shape["fs"] * across
    in_specs = (
        P("rep", None),
        P("rep", None),
        P(None, PLANE),
        P(None, PLANE),
        P(PLANE, None),
    )
    out_specs = (
        P("rep", None),
        P("rep", PLANE),
        P("rep", PLANE),
        P(PLANE, "rep"),
    )
    body = functools.partial(local, mesh.shape["rep"], chips, across)
    return jax.shard_map(body, mesh=mesh, in_specs=in_specs, out_specs=out_specs, check_vma=False)
```

profile of v0, /device:TPU:0, one launch (start us, length us, event | category | flops | bytes accessed | tf_op | source)
XLA Modules:
  0.0 142.3 jit_solution(7572952296496078483)
XLA Ops:
  0.6 0.0 slice-start
  0.7 55.2 %token_gather.1 = (bf16[4,4,32,4096]{3,2,1,0:T(8,128)(2,1)}, bf16[4,4,32,4096]{3,2,1,0:T(8,128)(2,1)}) custom-call(bf16[4,32,4096]{2,1,0:T(8,128)(2,1)} %bitcast.22, bf16[4,32,4096]{2,1,0:T(8,128)(2,1)} %bitcast.23), custom_call_target="tpu_custom_call" | custom-call | tf_op jit(solution)/shard_map/token_gather/pallas_call | solution.py:109
  55.9 0.0 slice-start.1
  55.9 0.0 slice-start.2
  55.9 0.0 copy-start.1
  55.9 12.1 %fusion.19 = f32[512,1408]{1,0:T(8,128)} fusion(bf16[512,4096]{1,0:T(8,128)(2,1)} %bitcast.24, bf16[4096,1408]{1,0:T(8,128)(2,1)} %param.7), kind=kOutput, calls=%fused_computation.23 | convolution fusion | flops 5905580032 | bytes 18612224 | tf_op jit(solution)/shard_map/dot_general | solution.py:202
  68.0 0.0 slice-done
  68.0 0.0 slice-done.1
  68.0 0.0 slice-done.2
  68.0 0.0 copy-done.1
  68.0 8.3 %fusion.18 = f32[512,1408]{1,0:T(8,128)} fusion(bf16[512,4096]{1,0:T(8,128)(2,1)S(1)} %bitcast.27, bf16[4096,1408]{1,0:T(8,128)(2,1)S(1)} %bitcast.19), kind=kOutput, calls=%fused_computation.22 | convolution fusion | flops 5905580032 | bytes 18612224 | tf_op jit(solution)/shard_map/dot_general | solution.py:203
  76.3 0.0 copy-start.2
  76.3 14.8 %multiply_convert_fusion.1 = (bf16[512,1408]{1,0:T(8,128)(2,1)S(1)}, bf16[512,1408]{1,0:T(8,128)(2,1)}) fusion(f32[512,1408]{1,0:T(8,128)} %fusion.19, f32[512,1408]{1,0:T(8,128)} %fusion.18, bf16[512,4096]{1,0:T(8,128)(2,1)} %bitcast.28, bf16[1408,4096]{1,0:T(8,128)(2,1)} %param.9), kind=kOutput, calls=%fused_computation.3 | convolution fusion | flops 5914951680 | bytes 24379392 | tf_op jit(solution)/shard_map/dot_general | solution.py:21
  91.0 0.0 copy-done.2
  91.1 0.0 slice-start.3
  91.1 0.0 slice-start.4
  91.1 6.6 %fusion.2 = f32[1408,1024]{1,0:T(8,128)} fusion(f32[512,1408]{1,0:T(8,128)} %fusion.18, bf16[512,4096]{1,0:T(8,128)(2,1)} %bitcast.29, s32[]{:T(128)S(6)} %select_n.9, f32[512,1408]{1,0:T(8,128)S(1)} %copy-done.2), kind=kOutput, calls=%fused_computation.7 | convolution fusion | flops 1480720384 | bytes 12582916 | tf_op jit(solution)/shard_map/dot_general | solution.py:15
  97.6 0.0 slice-start.5
  97.6 8.3 %fusion.10 = f32[128,4096]{1,0:T(8,128)S(1)} fusion(bf16[4096,1408]{1,0:T(8,128)(2,1)} %param.7, bf16[512,1408]{1,0:T(8,128)(2,1)} %get-tuple-element.9, s32[]{:T(128)S(6)} %select_n.8), kind=kOutput, calls=%fused_computation.14 | convolution fusion | flops 1476395008 | bytes 13991940 | tf_op jit(solution)/shard_map/dot_general | solution.py:21
  106.0 0.0 slice-done.3
  106.0 0.0 slice-done.4
  106.0 0.0 slice-done.5
  106.0 3.8 %fusion = bf16[128,4096]{1,0:T(8,128)(2,1)S(1)} fusion(f32[128,4096]{1,0:T(8,128)S(1)} %fusion.10, bf16[4096,1408]{1,0:T(8,128)(2,1)S(1)} %bitcast.21, bf16[512,1408]{1,0:T(8,128)(2,1)S(1)} %get-tuple-element.8, s32[]{:T(128)S(6)} %select_n.8), kind=kOutput, calls=%fused_computation.1 | convolution fusion | flops 1477443584 | bytes 15040516 | tf_op jit(solution)/shard_map/dot_general | solution.py:21
  109.8 20.1 %plane_sum.1 = bf16[4,2,16,4096]{3,2,1,0:T(8,128)(2,1)S(1)} custom-call(bf16[4,2,16,4096]{3,2,1,0:T(8,128)(2,1)S(1)} %bitcast.16), custom_call_target="tpu_custom_call" | custom-call | tf_op jit(solution)/shard_map/plane_sum/pallas_call | solution.py:178
  129.9 0.0 copy-start
  129.9 5.7 %fusion.4 = f32[1024,1408]{1,0:T(8,128)} fusion(bf16[512,1408]{1,0:T(8,128)(2,1)S(1)} %get-tuple-element.8, bf16[512,4096]{1,0:T(8,128)(2,1)} %bitcast.25, s32[]{:T(128)S(6)} %select_n.9), kind=kOutput, calls=%fused_computation.9 | convolution fusion | flops 1476395008 | bytes 8257540 | tf_op jit(solution)/shard_map/dot_general | solution.py:15
  135.7 0.0 copy-done
  135.7 5.6 %fusion.6 = f32[1024,1408]{1,0:T(8,128)} fusion(bf16[512,1408]{1,0:T(8,128)(2,1)S(1)} %copy-done, bf16[512,4096]{1,0:T(8,128)(2,1)} %bitcast.26, s32[]{:T(128)S(6)} %select_n.9), kind=kOutput, calls=%fused_computation.11 | convolution fusion | flops 1476395008 | bytes 8257540 | tf_op jit(solution)/shard_map/dot_general | solution.py:15
  141.3 1.0 copy.10
  (2 shorter events, 0.0 us)
Async XLA Ops:
  0.6 67.4 %slice-start = ((s8[11534336]{0:T(1024)(128)(4,1)}), s8[3145728]{0:T(1024)(128)(4,1)S(1)}, s32[]{:S(2)}) async-start(s8[11534336]{0:T(1024)(128)(4,1)} %bitcast.18), calls=%async_computation | async-start | bytes 6291456
  55.9 12.1 %slice-start.1 = ((s8[11534336]{0:T(1024)(128)(4,1)}), s8[4194304]{0:T(1024)(128)(4,1)S(1)}, s32[]{:S(2)}) async-start(s8[11534336]{0:T(1024)(128)(4,1)} %bitcast.18), calls=%async_computation.1 | async-start | bytes 8388608
  55.9 12.1 %slice-start.2 = ((s8[11534336]{0:T(1024)(128)(4,1)}), s8[4194304]{0:T(1024)(128)(4,1)S(1)}, s32[]{:S(2)}) async-start(s8[11534336]{0:T(1024)(128)(4,1)} %bitcast.18), calls=%async_computation.2 | async-start | bytes 8388608
  55.9 12.1 %copy-start.1 = (bf16[4,4,32,4096]{3,2,1,0:T(8,128)(2,1)S(1)}, bf16[4,4,32,4096]{3,2,1,0:T(8,128)(2,1)}, u32[]{:S(2)}) copy-start(bf16[4,4,32,4096]{3,2,1,0:T(8,128)(2,1)} %get-tuple-element.7) | copy-start | bytes 12582916
  76.3 14.8 %copy-start.2 = (f32[512,1408]{1,0:T(8,128)S(1)}, f32[512,1408]{1,0:T(8,128)}, u32[]{:S(2)}) copy-start(f32[512,1408]{1,0:T(8,128)} %fusion.19) | copy-start | bytes 8650756
  91.1 14.9 %slice-start.3 = ((s8[11534336]{0:T(1024)(128)(4,1)}), s8[4194304]{0:T(1024)(128)(4,1)S(1)}, s32[]{:S(2)}) async-start(s8[11534336]{0:T(1024)(128)(4,1)} %bitcast.20), calls=%async_computation.3 | async-start | bytes 8388608
  91.1 14.9 %slice-start.4 = ((s8[11534336]{0:T(1024)(128)(4,1)}), s8[4194304]{0:T(1024)(128)(4,1)S(1)}, s32[]{:S(2)}) async-start(s8[11534336]{0:T(1024)(128)(4,1)} %bitcast.20), calls=%async_computation.4 | async-start | bytes 8388608
  97.6 8.3 %slice-start.5 = ((s8[11534336]{0:T(1024)(128)(4,1)}), s8[3145728]{0:T(1024)(128)(4,1)S(1)}, s32[]{:S(2)}) async-start(s8[11534336]{0:T(1024)(128)(4,1)} %bitcast.20), calls=%async_computation.5 | async-start | bytes 6291456
  129.9 5.7 %copy-start = (bf16[512,1408]{1,0:T(8,128)(2,1)S(1)}, bf16[512,1408]{1,0:T(8,128)(2,1)}, u32[]{:S(2)}) copy-start(bf16[512,1408]{1,0:T(8,128)(2,1)} %get-tuple-element.9) | copy-start | bytes 4325380
where the time goes:
time: 142 us
  Pallas kernels  75.4 us (53%)
  matrix products  65.1 us (46%)
    pallas_call x1, Pallas kernels, gather(): pl.pallas_call(functools.partial(gather_kernel, reps), out_shape=(whole,...  55.2 us
    dot_general x3, matrix products, contract_cols(): lax.dot_general(left, right, (((1,), (1,)), ((), ())), preferred_element_...  26.8 us
    pallas_call x1, Pallas kernels, plane_sum(): pl.pallas_call(functools.partial(reduce_kernel, chips, across), out_shape...  20.1 us
    dot_general x3, matrix products, contract_rows(): lax.dot_general(left, right, (((0,), (0,)), ((), ())), preferred_element_...  17.9 us
    dot_general x1, matrix products, local(): gate_pre = jnp.dot(all_inputs, w_gate, preferred_element_type=jnp.float32)  12.1 us
    dot_general x1, matrix products, local(): up_pre = jnp.dot(all_inputs, w_upward, preferred_element_type=jnp.float32)  8.26 us

commit v1 on v0

--- a/solution.py
+++ b/solution.py
@@ -195,8 +195,356 @@
     return total.reshape(rows, width)
 
 
+def chunks_of(total, width):
+    return [(at, min(width, total - at)) for at in range(0, total, width)]
+
+
+def fused_kernel(
+    reps, chips, across, x_hbm, c_hbm, wg_hbm, wu_hbm, wd_hbm,
+    out, hid, gd, ud, xc, cc,
+    all_x, all_c, wg, wu, wd, gpre, upre, terms, got, sums, landed,
+    send, recv, sum_send, sum_recv, local_sem, weight_sem,
+):
+    z, y, t = lax.axis_index("rep"), lax.axis_index("fs"), lax.axis_index("tp")
+    x, core = t // 2, t % 2
+    rows, width = all_x.shape[1:]
+    hidden = wg.shape[1]
+    quarter = rows // 4
+    cols = width // reps
+    half = (x + y) % 2
+    mine = 2 * half + core
+    over = 2 * (1 - half) + core
+    chip = y * across + x
+    x_near = (z, y, 2 * (x + 1 - 2 * (x % 2)) + core)
+    y_near = (z, y + 1 - 2 * (y % 2), t)
+    other = (z, y, 2 * x + 1 - core)
+    pieces = chunks_of(hidden, 512)
+
+    def peer(ahead):
+        there = (chip + ahead) % chips
+        return there, (z, there // across, 2 * (there % across) + core)
+
+    def rows_of(part):
+        return pl.ds(pl.multiple_of(part * quarter, quarter), quarter)
+
+    local = [
+        pltpu.make_async_copy(x_hbm, all_x.at[z], local_sem.at[0]),
+        pltpu.make_async_copy(c_hbm, all_c.at[z], local_sem.at[1]),
+    ]
+    for copy in local:
+        copy.start()
+    weights = []
+    for at, size in pieces:
+        n = len(weights)
+        span = pl.ds(at, size)
+        weights.append([
+            pltpu.make_async_copy(wg_hbm.at[:, span], wg.at[:, span], weight_sem.at[n, 0]),
+            pltpu.make_async_copy(wu_hbm.at[:, span], wu.at[:, span], weight_sem.at[n, 1]),
+            pltpu.make_async_copy(wd_hbm.at[span], wd.at[span], weight_sem.at[n, 2]),
+        ])
+        for copy in weights[-1]:
+            copy.start()
+
+    greet(
+        [((z + 1) % reps, y, t), ((z + reps - 1) % reps, y, t), other]
+        + [peer(ahead)[1] for ahead in range(1, chips)]
+    )
+
+    def make(kind, block, src, dst, device, sender=None):
+        return pltpu.make_async_remote_copy(
+            src_ref=src, dst_ref=dst, send_sem=send.at[kind if sender is None else sender, block],
+            recv_sem=recv.at[kind, block], device_id=device, device_id_type=MESH,
+        )
+
+    started = []
+
+    def put(condition, copy):
+        if condition is None:
+            copy.start()
+        else:
+            pl.when(condition)(copy.start)
+        started.append((condition, copy))
+        return copy
+
+    own = rows_of(mine)
+    for kind, src, dst in ((0, x_hbm, all_x), (1, c_hbm, all_c)):
+        put(z < reps - 1, make(kind, z, src.at[own], dst.at[z, own], (jnp.minimum(z + 1, reps - 1), y, t)))
+        put(z > 0, make(kind, z, src.at[own], dst.at[z, own], (jnp.maximum(z - 1, 0), y, t), 8 + kind))
+
+    def sides(step):
+        low, high = z - 1 - step, z + 1 + step
+        return (
+            (low >= 0, jnp.maximum(low, 0), jnp.minimum(z + 1, reps - 1), (low >= 0) & (z < reps - 1)),
+            (high < reps, jnp.minimum(high, reps - 1), jnp.maximum(z - 1, 0), (high < reps) & (z > 0)),
+        )
+
+    def guarded(condition, action):
+        pl.when(condition)(action)
+
+    def hop(array, step):
+        buffer = (all_x, all_c)[array]
+        near = (x_near, y_near)[array]
+        for valid, block, onward, passes in sides(step):
+            piece = buffer.at[block, own]
+            arrived = make(array, block, piece, piece, other)
+            guarded(valid, arrived.wait_recv)
+            put(passes, make(array, block, piece, piece, (onward, y, t)))
+            put(valid, make(2 + array, block, piece, piece, near))
+            put(valid, make(4 + array, block, piece, piece, other))
+
+    def relay(array, step):
+        buffer = (all_x, all_c)[array]
+        far = rows_of(over)
+        for valid, block, _, _ in sides(step):
+            piece = buffer.at[block, far]
+            arrived = make(2 + array, block, piece, piece, other)
+            guarded(valid, arrived.wait_recv)
+            put(valid, make(6 + array, block, piece, piece, other))
+
+    def complete(array, block):
+        buffer = (all_x, all_c)[array]
+        for kind in (4, 6):
+            piece = buffer.at[block, own]
+            make(kind + array, block, piece, piece, other).wait_recv()
+
+    def pre(block, at, size):
+        span = pl.ds(at, size)
+        tokens = all_x[block]
+        gpre[:, span] = jnp.dot(tokens, wg[:, span], preferred_element_type=jnp.float32)
+        upre[:, span] = jnp.dot(tokens, wu[:, span], preferred_element_type=jnp.float32)
+
+    def deltas(block, at, size):
+        span = pl.ds(at, size)
+        grad = contract_cols(all_c[block], wd[span, :])
+        gate, up = gpre[:, span], upre[:, span]
+        sig = jax.nn.sigmoid(gate)
+        act = gate * sig
+        hid[block, :, span] = (act * up).astype(hid.dtype)
+        gd[block, :, span] = (grad * up * sig * (1.0 + gate * (1.0 - sig))).astype(gd.dtype)
+        ud[block, :, span] = (grad * act).astype(ud.dtype)
+
+    def keep_cols(array, block):
+        span = pl.ds(pl.multiple_of(z * cols, cols), cols)
+        source, target = ((all_x, xc), (all_c, cc))[array]
+        target[block] = source[block, :, span]
+
+    for copy in local:
+        copy.wait()
+    for n, (at, size) in enumerate(pieces):
+        weights[n][0].wait()
+        weights[n][1].wait()
+        pre(z, at, size)
+        weights[n][2].wait()
+        deltas(z, at, size)
+        if n == 1:
+            hop(0, 0)
+
+    part = width // 4
+    for n in range(4):
+        span = pl.ds(n * part, part)
+        term = contract_cols(gd[z], wg[span, :]) + contract_cols(ud[z], wu[span, :])
+        term = term.astype(terms.dtype)
+        terms[..., span] = term.reshape(terms.shape[:-1] + (part,))
+        if n == 0:
+            hop(1, 0)
+        if n == 2:
+            relay(0, 0)
+
+    def sum_copy(kind, slot, src, dst, device):
+        return pltpu.make_async_remote_copy(
+            src_ref=src, dst_ref=dst, send_sem=sum_send.at[kind, slot],
+            recv_sem=sum_recv.at[kind, slot], device_id=device, device_id_type=MESH,
+        )
+
+    swaps = [put(None, sum_copy(0, j, terms.at[j, 1 - core], got.at[j], other)) for j in range(chips)]
+    hop(0, 1)
+    relay(1, 0)
+
+    def reduce_first():
+        for j in range(chips):
+            swaps[j].wait_recv()
+            pair = terms[j, core].astype(jnp.float32) + got[j].astype(jnp.float32)
+            sums[j] = pair.astype(sums.dtype)
+        spread = []
+        for ahead in range(1, chips):
+            there, device = peer(ahead)
+            spread.append(put(None, sum_copy(1, ahead, sums.at[there], landed.at[ahead], device)))
+        return spread
+
+    done = out.at[chip, core]
+
+    def reduce_second(spread):
+        total = terms[chip, core].astype(jnp.float32) + got[chip].astype(jnp.float32)
+        for ahead in range(1, chips):
+            spread[ahead - 1].wait_recv()
+            total = total + landed[ahead].astype(jnp.float32)
+        out[chip, core] = total.astype(out.dtype)
+        share = [put(None, sum_copy(2, ahead, done, done, peer(ahead)[1])) for ahead in range(1, chips)]
+        relays = [put(None, sum_copy(3, 0, done, done, other))]
+        return share, relays
+
+    def reduce_third(share, relays):
+        for ahead in range(1, chips):
+            share[ahead - 1].wait_recv()
+            source = out.at[(chip + chips - ahead) % chips, core]
+            relays.append(put(None, sum_copy(3, ahead, source, source, other)))
+
+    fewer = jnp.minimum(z, reps - 1 - z)
+
+    def order(turn):
+        step = jnp.where(turn < 2 * fewer, turn // 2, turn - fewer)
+        low = jnp.where(turn < 2 * fewer, turn % 2 == 0, z > reps - 1 - z)
+        return jnp.where(low, z - 1 - step, z + 1 + step)
+
+    keep_cols(0, z)
+    keep_cols(1, z)
+    share = relays = spread = None
+    for turn in range(reps - 1):
+        block = order(turn)
+        complete(0, block)
+        keep_cols(0, block)
+        for n, (at, size) in enumerate(pieces):
+            pre(block, at, size)
+        if turn == 0:
+            spread = reduce_first()
+        if turn == 1:
+            share, relays = reduce_second(spread)
+        if turn + 1 < reps - 1:
+            hop(1, turn + 1)
+            relay(0, turn + 1)
+        complete(1, block)
+        keep_cols(1, block)
+        for n, (at, size) in enumerate(pieces):
+            deltas(block, at, size)
+        if turn + 2 < reps - 1:
+            hop(0, turn + 2)
+        if turn + 1 < reps - 1:
+            relay(1, turn + 1)
+        if turn == 1:
+            reduce_third(share, relays)
+    for copy in relays:
+        copy.wait_recv()
+    for condition, copy in started:
+        if condition is None:
+            copy.wait_send()
+        else:
+            guarded(condition, copy.wait_send)
+
+
+def fused(reps, chips, across, inputs, cotangent, w_gate, w_upward, w_down):
+    rows, width = inputs.shape
+    hidden = w_gate.shape[1]
+    cols = width // reps
+    kind = inputs.dtype
+    piece = (rows // (2 * chips), width)
+    vmem = pl.BlockSpec(memory_space=pltpu.VMEM)
+    anywhere = pl.BlockSpec(memory_space=pl.ANY)
+    count = len(chunks_of(hidden, 512))
+    wide = jax.ShapeDtypeStruct((reps, rows, hidden), kind)
+    slim = jax.ShapeDtypeStruct((reps, rows, cols), kind)
+    total, hid, gd, ud, xc, cc = pl.pallas_call(
+        functools.partial(fused_kernel, reps, chips, across),
+        out_shape=(jax.ShapeDtypeStruct((chips, 2) + piece, kind), wide, wide, wide, slim, slim),
+        in_specs=[anywhere] * 5,
+        out_specs=(vmem,) * 6,
+        scratch_shapes=[
+            pltpu.VMEM((reps, rows, width), kind),
+            pltpu.VMEM((reps, rows, width), kind),
+            pltpu.VMEM((width, hidden), kind),
+            pltpu.VMEM((width, hidden), kind),
+            pltpu.VMEM((hidden, width), kind),
+            pltpu.VMEM((rows, hidden), jnp.float32),
+            pltpu.VMEM((rows, hidden), jnp.float32),
+            pltpu.VMEM((chips, 2) + piece, kind),
+            pltpu.VMEM((chips,) + piece, kind),
+            pltpu.VMEM((chips,) + piece, kind),
+            pltpu.VMEM((chips,) + piece, kind),
+            pltpu.SemaphoreType.DMA((10, reps)),
+            pltpu.SemaphoreType.DMA((8, reps)),
+            pltpu.SemaphoreType.DMA((4, chips)),
+            pltpu.SemaphoreType.DMA((4, chips)),
+            pltpu.SemaphoreType.DMA((2,)),
+            pltpu.SemaphoreType.DMA((count, 3)),
+        ],
+        compiler_params=pltpu.CompilerParams(
+            collective_id=2, has_side_effects=True, vmem_limit_bytes=63 * 2**20
+        ),
+        name="gather_compute",
+    )(inputs, cotangent, w_gate, w_upward, w_down)
+    return total.reshape(rows, width), [a.reshape(reps * rows, -1) for a in (hid, gd, ud, xc, cc)]
+
+
+def weights_kernel(tall, wide_rows, hid, gd, ud, xc, cc, total, g_gate, g_up, g_down, g_in, stage, stage_down, sems, down_sems, in_sem):
+    whole = pltpu.make_async_copy(total, g_in, in_sem)
+    whole.start()
+    pending = [None] * stage.shape[0]
+    turn = 0
+    for delta, target in ((gd, g_gate), (ud, g_up)):
+        for at, size in chunks_of(xc.shape[1], tall):
+            slot = turn % len(pending)
+            if pending[slot] is not None:
+                pending[slot].wait()
+            span = pl.ds(at, size)
+            stage[slot, :size] = contract_rows(xc[:, span], delta[...])
+            pending[slot] = pltpu.make_async_copy(stage.at[slot, pl.ds(0, size)], target.at[span], sems.at[slot])
+            pending[slot].start()
+            turn += 1
+    later = [None] * stage_down.shape[0]
+    turn = 0
+    for at, size in chunks_of(hid.shape[1], wide_rows):
+        slot = turn % len(later)
+        if later[slot] is not None:
+            later[slot].wait()
+        span = pl.ds(at, size)
+        stage_down[slot, :size] = contract_rows(hid[:, span], cc[...])
+        later[slot] = pltpu.make_async_copy(stage_down.at[slot, pl.ds(0, size)], g_down.at[span], down_sems.at[slot])
+        later[slot].start()
+        turn += 1
+    for copy in pending + later:
+        if copy is not None:
+            copy.wait()
+    whole.wait()
+
+
+def weight_gradients(total, hid, gd, ud, xc, cc):
+    hidden, cols = hid.shape[1], xc.shape[1]
+    vmem = pl.BlockSpec(memory_space=pltpu.VMEM)
+    anywhere = pl.BlockSpec(memory_space=pl.ANY)
+    up = jax.ShapeDtypeStruct((cols, hidden), jnp.float32)
+    down = jax.ShapeDtypeStruct((hidden, cols), jnp.float32)
+    tall, wide_rows, slots = 256, 384, 3
+    return pl.pallas_call(
+        functools.partial(weights_kernel, tall, wide_rows),
+        out_shape=(up, up, down, jax.ShapeDtypeStruct(total.shape, total.dtype)),
+        in_specs=[vmem] * 6,
+        out_specs=(anywhere,) * 4,
+        scratch_shapes=[
+            pltpu.VMEM((slots, tall, hidden), jnp.float32),
+            pltpu.VMEM((slots, wide_rows, cols), jnp.float32),
+            pltpu.SemaphoreType.DMA((slots,)),
+            pltpu.SemaphoreType.DMA((slots,)),
+            pltpu.SemaphoreType.DMA,
+        ],
+        compiler_params=pltpu.CompilerParams(vmem_limit_bytes=40 * 2**20),
+        name="weight_gradients",
+    )(hid, gd, ud, xc, cc, total)
+
+
+def fits(reps, chips, across, inputs, w_gate):
+    rows, width = inputs.shape
+    hidden = w_gate.shape[1]
+    size = inputs.dtype.itemsize
+    need = size * (3 * width * hidden + 2 * reps * rows * width + 3 * reps * rows * hidden)
+    aligned = hidden % 128 == 0 and width % (128 * reps) == 0 and rows % 64 == 0
+    return aligned and chips == 4 and across == 2 and need < 52 * 2**20
+
+
 def local(reps, chips, across, inputs, cotangent, w_gate, w_upward, w_down):
     rows, width = inputs.shape
+    if fits(reps, chips, across, inputs, w_gate):
+        total, parts = fused(reps, chips, across, inputs, cotangent, w_gate, w_upward, w_down)
+        grad_gate, grad_upward, grad_down, grad_input = weight_gradients(total, *parts)
+        return (grad_input, grad_gate, grad_upward, grad_down)
     all_inputs, all_cotangent = gather(reps, inputs, cotangent)
 
     gate_pre = jnp.dot(all_inputs, w_gate, preferred_element_type=jnp.float32)

time: 142 us -> 91.8 us (0.65)
  matrix products: 65.1 us -> 0 us
  Pallas kernels: 75.4 us -> 82.9 us
  local copies, waits for them, and re-layouts: 1.02 us -> 7.75 us
    dot_general x8 -> x0, matrix products: 65.1 us -> none  [the longest x3 26.8 us: contract_cols(): lax.dot_general(left, right, (((1,), (1,)), ((), ())), preferred_element_...]
    pallas_call x2, Pallas kernels: 75.4 us -> 82.9 us  [the longest x1 74.9 us: fused(): pl.pallas_call(functools.partial(fused_kernel, reps, chips, across), out_...]
    unnamed x19 -> x12, local copies, waits for them, and re-layouts: 1.02 us -> 7.75 us
where the time goes in v1:
time: 91.8 us; the launch traced here: 91.5 us
  Pallas kernels  82.9 us (90%)
  local copies, waits for them, and re-layouts  7.75 us (8%)
    pallas_call x1, Pallas kernels, fused(): pl.pallas_call(functools.partial(fused_kernel, reps, chips, across), out_...  74.9 us
    pallas_call x1, Pallas kernels, weight_gradients(): pl.pallas_call(functools.partial(weights_kernel, tall, wide_rows), out_sh...  8.01 us
    unnamed x12, local copies, waits for them, and re-layouts  7.75 us

profile of v1, /device:TPU:0, one launch (start us, length us, event | category | flops | bytes accessed | tf_op | source)
XLA Modules:
  0.0 91.5 jit_solution(4698890544497571147)
XLA Ops:
  0.6 74.9 %gather_compute.1 = (bf16[4,2,16,4096]{3,2,1,0:T(8,128)(2,1)}, bf16[4,128,1408]{2,1,0:T(8,128)(2,1)}, bf16[4,128,1408]{2,1,0:T(8,128)(2,1)}, bf16[4,128,1408]{2,...) custom-call(bf16[128,4096]{1,0:T(8,128)(2,1)} %x_hbm.1, bf16[128,4096]{1,0:T(8,128)(2,1)} %c_hbm.1, ...), custom_call_target="tpu_custom_call" | custom-call | tf_op jit(solution)/shard_map/gather_compute/pallas_call | solution.py:445
  75.5 0.0 copy-start
  75.5 1.4 %copy-done = bf16[4,128,1408]{2,1,0:T(8,128)(2,1)S(1)} copy-done((bf16[4,128,1408]{2,1,0:T(8,128)(2,1)S(1)}, bf16[4,128,1408]{2,1,0:T(8,128)(2,1)}, u32[]{:S(2)}) %copy-start) | copy-done | bytes 1441816
  76.9 0.0 copy-start.1
  76.9 1.4 %copy-done.1 = bf16[4,128,1408]{2,1,0:T(8,128)(2,1)S(1)} copy-done((bf16[4,128,1408]{2,1,0:T(8,128)(2,1)S(1)}, bf16[4,128,1408]{2,1,0:T(8,128)(2,1)}, u32[]{:S(2)}) %copy-start.1) | copy-done | bytes 1441816
  78.3 0.0 copy-start.2
  78.3 1.4 %copy-done.2 = bf16[4,128,1408]{2,1,0:T(8,128)(2,1)S(1)} copy-done((bf16[4,128,1408]{2,1,0:T(8,128)(2,1)S(1)}, bf16[4,128,1408]{2,1,0:T(8,128)(2,1)}, u32[]{:S(2)}) %copy-start.2) | copy-done | bytes 1441816
  79.6 0.0 copy-start.3
  79.6 1.2 %copy-done.3 = bf16[4,2,16,4096]{3,2,1,0:T(8,128)(2,1)S(1)} copy-done((bf16[4,2,16,4096]{3,2,1,0:T(8,128)(2,1)S(1)}, bf16[4,2,16,4096]{3,2,1,0:T(8,128)(2,1)}, u32[]{:S(2)}) %copy-start.3) | copy-done | bytes 1048600
  80.8 0.0 copy-start.4
  80.8 1.2 %copy-done.4 = bf16[4,128,1024]{2,1,0:T(8,128)(2,1)S(1)} copy-done((bf16[4,128,1024]{2,1,0:T(8,128)(2,1)S(1)}, bf16[4,128,1024]{2,1,0:T(8,128)(2,1)}, u32[]{:S(2)}) %copy-start.4) | copy-done | bytes 1048600
  82.1 0.0 copy-start.5
  82.1 1.2 %copy-done.5 = bf16[4,128,1024]{2,1,0:T(8,128)(2,1)S(1)} copy-done((bf16[4,128,1024]{2,1,0:T(8,128)(2,1)S(1)}, bf16[4,128,1024]{2,1,0:T(8,128)(2,1)}, u32[]{:S(2)}) %copy-start.5) | copy-done | bytes 1048600
  83.3 8.0 %weight_gradients.1 = (f32[1024,1408]{1,0:T(8,128)}, f32[1024,1408]{1,0:T(8,128)}, f32[1408,1024]{1,0:T(8,128)}, bf16[128,4096]{1,0:T(8,128)(2,1)}) custom-call(bf16[512,1408]{1,0:T(8,128)(2,1)S(1)} %bitcast.6, bf16[512,1408]{1,0:T(8,128)(2,1)S(1)} %bitcast.7, bf16[512,1408]{1,0:T(8,128)(2,1)S(1)} %bitcast.8, bf16[512,1024]{1,0:T(8,128)(2,1)S(1)} %bitcast.10, ...), custom_call_target="tpu_custom_call" | custom-call | tf_op jit(solution)/shard_map/weight_gradients/pallas_call | solution.py:516
Async XLA Ops:
  75.5 1.4 %copy-start = (bf16[4,128,1408]{2,1,0:T(8,128)(2,1)S(1)}, bf16[4,128,1408]{2,1,0:T(8,128)(2,1)}, u32[]{:S(2)}) copy-start(bf16[4,128,1408]{2,1,0:T(8,128)(2,1)} %get-tuple-element.14) | copy-start | bytes 4325380
  76.9 1.4 %copy-start.1 = (bf16[4,128,1408]{2,1,0:T(8,128)(2,1)S(1)}, bf16[4,128,1408]{2,1,0:T(8,128)(2,1)}, u32[]{:S(2)}) copy-start(bf16[4,128,1408]{2,1,0:T(8,128)(2,1)} %get-tuple-element.15) | copy-start | bytes 4325380
  78.3 1.4 %copy-start.2 = (bf16[4,128,1408]{2,1,0:T(8,128)(2,1)S(1)}, bf16[4,128,1408]{2,1,0:T(8,128)(2,1)}, u32[]{:S(2)}) copy-start(bf16[4,128,1408]{2,1,0:T(8,128)(2,1)} %get-tuple-element.16) | copy-start | bytes 4325380
  79.6 1.2 %copy-start.3 = (bf16[4,2,16,4096]{3,2,1,0:T(8,128)(2,1)S(1)}, bf16[4,2,16,4096]{3,2,1,0:T(8,128)(2,1)}, u32[]{:S(2)}) copy-start(bf16[4,2,16,4096]{3,2,1,0:T(8,128)(2,1)} %get-tuple-element.19) | copy-start | bytes 3145732
  80.8 1.2 %copy-start.4 = (bf16[4,128,1024]{2,1,0:T(8,128)(2,1)S(1)}, bf16[4,128,1024]{2,1,0:T(8,128)(2,1)}, u32[]{:S(2)}) copy-start(bf16[4,128,1024]{2,1,0:T(8,128)(2,1)} %get-tuple-element.17) | copy-start | bytes 3145732
  82.1 1.2 %copy-start.5 = (bf16[4,128,1024]{2,1,0:T(8,128)(2,1)S(1)}, bf16[4,128,1024]{2,1,0:T(8,128)(2,1)}, u32[]{:S(2)}) copy-start(bf16[4,128,1024]{2,1,0:T(8,128)(2,1)} %get-tuple-element.18) | copy-start | bytes 3145732

commit v2 on v0

--- a/solution.py
+++ b/solution.py
@@ -9,6 +9,9 @@
 
 PLANE = ("fs", "tp")
 MESH = pl.DeviceIdType.MESH
+STREAM = (256, 256, 512, 384)
+BLOCK = (512, 512, 384)
+FLIGHT = 4
 
 
 def contract_rows(left, right):
@@ -195,8 +198,462 @@
     return total.reshape(rows, width)
 
 
+def chunks_of(total, widths):
+    spans, at = [], 0
+    for width in widths:
+        if at < total:
+            spans.append((at, min(width, total - at)))
+            at += width
+    while at < total:
+        spans.append((at, min(widths[-1], total - at)))
+        at += widths[-1]
+    return spans
+
+
+def fused_kernel(
+    reps, chips, across, x_hbm, c_hbm, wg_hbm, wu_hbm, wd_hbm,
+    out, hid, gd, ud, xc, cc,
+    all_x, all_c, wg, wu, wd, gpre, upre, got, landed,
+    send, recv, sum_send, sum_recv, local_sem, weight_sem,
+):
+    z, y, t = lax.axis_index("rep"), lax.axis_index("fs"), lax.axis_index("tp")
+    x, core = t // 2, t % 2
+    rows, width = all_x.shape[1:]
+    hidden = wg.shape[1]
+    cols = width // reps
+    chip = y * across + x
+    x_chip, y_chip = y * across + 1 - x, (1 - y) * across + x
+    far_chip = (1 - y) * across + 1 - x
+    x_near, y_near = (z, y, 2 * (1 - x) + core), (z, 1 - y, t)
+    other = (z, y, 2 * x + 1 - core)
+    near = (z, jnp.where(core == 0, y, 1 - y), jnp.where(core == 0, 2 * (1 - x) + core, t))
+    crosswise = (z, jnp.where(core == 0, 1 - y, y), jnp.where(core == 0, t, 2 * (1 - x) + core))
+    half = (x + y) % 2
+
+    def peer(ahead):
+        there = (chip + ahead) % chips
+        return there, (z, there // across, 2 * (there % across) + core)
+
+    def part_of(parts, index):
+        size = rows // parts
+        return pl.ds(pl.multiple_of(index * size, size), size)
+
+    def x_part(of_chip, of_core):
+        return part_of(8, 2 * of_chip + of_core)
+
+    def c_part(of_half, of_core):
+        return part_of(4, 2 * of_half + of_core)
+
+    local = [
+        pltpu.make_async_copy(x_hbm, all_x.at[0], local_sem.at[0]),
+        pltpu.make_async_copy(c_hbm, all_c.at[0], local_sem.at[1]),
+    ]
+    for copy in local:
+        copy.start()
+    stream = chunks_of(hidden, STREAM)
+    weights = []
+    for n, (at, size) in enumerate(stream):
+        span = pl.ds(at, size)
+        weights += [
+            pltpu.make_async_copy(wg_hbm.at[:, span], wg.at[:, span], weight_sem.at[n, 0]),
+            pltpu.make_async_copy(wu_hbm.at[:, span], wu.at[:, span], weight_sem.at[n, 1]),
+            pltpu.make_async_copy(wd_hbm.at[span], wd.at[span], weight_sem.at[n, 2]),
+        ]
+    for copy in weights[:FLIGHT]:
+        copy.start()
+
+    def weight_ready(n):
+        weights[n].wait()
+        if n + FLIGHT < len(weights):
+            weights[n + FLIGHT].start()
+
+    greet(
+        [((z + 1) % reps, y, t), ((z + reps - 1) % reps, y, t), other]
+        + [peer(ahead)[1] for ahead in range(1, chips)]
+    )
+
+    def slot_of(level, block):
+        step = jnp.where(block < level, level - block, block - level) - 1
+        fewer = jnp.minimum(level, reps - 1 - level)
+        paired = 2 * step + jnp.where(block < level, 0, 1)
+        return 1 + jnp.where(step < fewer, paired, step + fewer)
+
+    def make(kind, slot, src, dst, device, sender=None, there=None):
+        return pltpu.make_async_remote_copy(
+            src_ref=src, dst_ref=dst, send_sem=send.at[kind if sender is None else sender, slot],
+            recv_sem=recv.at[kind, slot if there is None else there],
+            device_id=device, device_id_type=MESH,
+        )
+
+    def pass_on(buffer, kind, slot, part, device):
+        piece = buffer.at[slot, part]
+        return make(kind, slot, piece, piece, device)
+
+    def hop_on(buffer, kind, slot, part, device, there):
+        return make(kind, slot, buffer.at[slot, part], buffer.at[there, part], device, None, there)
+
+    above, below = jnp.minimum(z + 1, reps - 1), jnp.maximum(z - 1, 0)
+    up, down = (above, y, t), (below, y, t)
+
+    def first_sends():
+        sends = []
+        for kind, src, buffer, part in (
+            (0, x_hbm, all_x, x_part(chip, core)), (8, c_hbm, all_c, c_part(half, core))
+        ):
+            for wanted, device, level, sender in (
+                (z < reps - 1, up, above, kind), (z > 0, down, below, 12 + kind // 8)
+            ):
+                there = slot_of(level, z)
+                copy = make(kind, 0, src.at[part], buffer.at[there, part], device, sender, there)
+                sends.append((wanted, copy))
+        return sends
+
+    def sides(step):
+        low, high = z - 1 - step, z + 1 + step
+        from_low, from_high = jnp.maximum(low, 0), jnp.minimum(high, reps - 1)
+        return (
+            (low >= 0, slot_of(z, from_low), up, slot_of(above, from_low), (low >= 0) & (z < reps - 1)),
+            (high < reps, slot_of(z, from_high), down, slot_of(below, from_high), (high < reps) & (z > 0)),
+        )
+
+    def hops(buffer, kind, part, step):
+        for valid, slot, onward, there, passes in sides(step):
+            yield valid, pass_on(buffer, kind, slot, part, other), passes, hop_on(buffer, kind, slot, part, onward, there)
+
+    def hop(array, step):
+        buffer, kind, part = ((all_x, 0, x_part(chip, core)), (all_c, 8, c_part(half, core)))[array]
+        for valid, arrived, passes, onward in hops(buffer, kind, part, step):
+            pl.when(valid)(arrived.wait_recv)
+            pl.when(passes)(onward.start)
+
+    beside, across_y, opposite = x_part(x_chip, core), x_part(y_chip, core), x_part(far_chip, core)
+    turned = part_of(8, 2 * jnp.where(core == 0, x_chip, y_chip) + core)
+
+    def near_x(slot):
+        part = x_part(chip, core)
+        return [
+            pass_on(all_x, 1, slot, part, x_near), pass_on(all_x, 2, slot, part, y_near),
+            pass_on(all_x, 4, slot, part, other),
+        ]
+
+    def spread_x(slot):
+        return [
+            pass_on(all_x, 3, slot, turned, crosswise), pass_on(all_x, 5, slot, beside, other),
+            pass_on(all_x, 6, slot, across_y, other),
+        ]
+
+    def last_x(slot):
+        return [pass_on(all_x, 7, slot, opposite, other)]
+
+    def near_c(slot):
+        part = c_part(half, core)
+        return [pass_on(all_c, 9, slot, part, near), pass_on(all_c, 10, slot, part, other)]
+
+    def last_c(slot):
+        return [pass_on(all_c, 11, slot, c_part(1 - half, core), other)]
+
+    awaited = {
+        near_x: (), near_c: (), spread_x: ((1, beside), (2, across_y)), last_x: ((3, opposite),),
+        last_c: ((9, c_part(1 - half, core)),),
+    }
+
+    def serve(service, slot):
+        buffer = all_c if service in (near_c, last_c) else all_x
+        for kind, part in awaited[service]:
+            pass_on(buffer, kind, slot, part, other).wait_recv()
+        for copy in service(slot):
+            copy.start()
+
+    def complete_x(slot):
+        for kind in range(4, 8):
+            pass_on(all_x, kind, slot, x_part(chip, core), other).wait_recv()
+        keep_cols(all_x, xc, slot)
+
+    def complete_c(slot):
+        for kind in range(10, 12):
+            pass_on(all_c, kind, slot, c_part(half, core), other).wait_recv()
+        keep_cols(all_c, cc, slot)
+
+    def pre(slot, place, at, size):
+        span, held = pl.ds(at, size), pl.ds(place * rows, rows)
+        tokens = all_x[slot]
+        gpre[held, span] = jnp.dot(tokens, wg[:, span], preferred_element_type=jnp.float32)
+        upre[held, span] = jnp.dot(tokens, wu[:, span], preferred_element_type=jnp.float32)
+
+    def deltas(slot, count, at, size):
+        span, held, slots = pl.ds(at, size), pl.ds(0, count * rows), pl.ds(slot, count)
+        tokens = all_c[slots].reshape(count * rows, width)
+        grad = contract_cols(tokens, wd[span, :])
+        gate, lift = gpre[held, span], upre[held, span]
+        sig = jax.nn.sigmoid(gate)
+        act = gate * sig
+        shape = (count, rows, size)
+        hid[slots, :, span] = (act * lift).astype(hid.dtype).reshape(shape)
+        gate_grad = grad * lift * sig * (1.0 + gate * (1.0 - sig))
+        gd[slots, :, span] = gate_grad.astype(gd.dtype).reshape(shape)
+        ud[slots, :, span] = (grad * act).astype(ud.dtype).reshape(shape)
+
+    def keep_cols(buffer, kept, slot):
+        span = pl.ds(pl.multiple_of(z * cols, cols), cols)
+        kept[slot] = buffer[slot, :, span]
+
+    small = rows // (2 * chips)
+
+    def term(piece, of_core):
+        return all_c.at[0, part_of(2 * chips, 2 * piece + of_core)]
+
+    def pair_sum(ahead):
+        return all_x.at[0, pl.ds((ahead - 1) * small, small)]
+
+    def sum_copy(kind, slot, src, dst, device):
+        return pltpu.make_async_remote_copy(
+            src_ref=src, dst_ref=dst, send_sem=sum_send.at[kind, slot],
+            recv_sem=sum_recv.at[kind, slot], device_id=device, device_id_type=MESH,
+        )
+
+    def swaps():
+        return [sum_copy(0, j, term(j, 1 - core), got.at[j], other) for j in range(chips)]
+
+    def spread():
+        return [
+            sum_copy(1, ahead, pair_sum(ahead), landed.at[ahead - 1], peer(ahead)[1])
+            for ahead in range(1, chips)
+        ]
+
+    def share():
+        done = out.at[chip, core]
+        return [sum_copy(2, ahead, done, done, peer(ahead)[1]) for ahead in range(1, chips)]
+
+    def relays():
+        sources = [out.at[(chip + chips - ahead) % chips, core] for ahead in range(chips)]
+        return [sum_copy(3, ahead, source, source, other) for ahead, source in enumerate(sources)]
+
+    def reduce_first():
+        for copy in swaps():
+            copy.wait_recv()
+        for ahead in range(1, chips):
+            there = peer(ahead)[0]
+            pair = term(there, core)[...].astype(jnp.float32) + got[there].astype(jnp.float32)
+            pair_sum(ahead)[...] = pair.astype(got.dtype)
+        for ahead, copy in enumerate(spread(), 1):
+            pl.when(peer(ahead)[0] != far_chip)(copy.start)
+
+    def diagonal():
+        for ahead, copy in enumerate(spread(), 1):
+            pl.when(peer(ahead)[0] == far_chip)(copy.start)
+
+    def reduce_second():
+        total = term(chip, core)[...].astype(jnp.float32) + got[chip].astype(jnp.float32)
+        for ahead, copy in enumerate(spread()):
+            copy.wait_recv()
+            total = total + landed[ahead].astype(jnp.float32)
+        out[chip, core] = total.astype(out.dtype)
+        for copy in share():
+            copy.start()
+        relays()[0].start()
+
+    def reduce_third():
+        for copy, onward in zip(share(), relays()[1:]):
+            copy.wait_recv()
+            onward.start()
+
+    for condition, copy in first_sends():
+        pl.when(condition)(copy.start)
+    for copy in local:
+        copy.wait()
+    keep_cols(all_x, xc, 0)
+    keep_cols(all_c, cc, 0)
+    slots = {
+        (0, 1): ((hop, 0, 0), (serve, near_x, 1)),
+        (1, 2): ((serve, spread_x, 1), (hop, 1, 0), (serve, near_c, 1)),
+        (1, 3): ((hop, 0, 1), (serve, near_x, 2)),
+        (2, 0): ((serve, last_x, 1),),
+        (2, 2): ((serve, last_c, 1), (hop, 1, 1), (serve, near_c, 2)),
+        (2, 3): ((serve, spread_x, 2),),
+        (3, 0): ((hop, 0, 2), (serve, near_x, 3)),
+        (3, 2): ((serve, last_x, 2),),
+        (4, 0): ((serve, last_c, 2),),
+        (4, 1): ((serve, spread_x, 3), (diagonal,)),
+        (4, 2): ((hop, 1, 2), (serve, near_c, 3)),
+        (5, 2): ((serve, last_x, 3),),
+        (6, 1): ((serve, last_c, 3), (reduce_second,)),
+    }
+
+    def at_slot(phase, n):
+        for action, *details in slots.get((phase, n), ()):
+            action(*details)
+
+    for n, (at, size) in enumerate(stream):
+        weight_ready(3 * n)
+        weight_ready(3 * n + 1)
+        pre(0, 0, at, size)
+        at_slot(0, n)
+        weight_ready(3 * n + 2)
+        deltas(0, 1, at, size)
+        at_slot(1, n)
+
+    part = width // 4
+    for n in range(4):
+        span = pl.ds(n * part, part)
+        total = contract_cols(gd[0], wg[span, :]) + contract_cols(ud[0], wu[span, :])
+        all_c[0, :, span] = total.astype(all_c.dtype)
+        at_slot(2, n)
+    for copy in swaps():
+        copy.start()
+
+    blocks = chunks_of(hidden, BLOCK)
+    complete_x(1)
+    for n, (at, size) in enumerate(blocks):
+        pre(1, 0, at, size)
+        at_slot(3, n)
+        if n == 1:
+            reduce_first()
+    complete_c(1)
+    for n, (at, size) in enumerate(blocks):
+        deltas(1, 1, at, size)
+        at_slot(4, n)
+    complete_x(2)
+    for n, (at, size) in enumerate(blocks):
+        pre(2, 0, at, size)
+        at_slot(5, n)
+    complete_x(3)
+    for n, (at, size) in enumerate(blocks):
+        pre(3, 1, at, size)
+        at_slot(6, n)
+    complete_c(2)
+    complete_c(3)
+    for n, (at, size) in enumerate(blocks):
+        deltas(2, 2, at, size)
+    reduce_third()
+    for copy in relays():
+        copy.wait_recv()
+    for condition, copy in first_sends():
+        pl.when(condition)(copy.wait_send)
+    for copy in swaps() + spread() + share() + relays():
+        copy.wait_send()
+
+    for slot in range(1, reps):
+        for service in (near_x, spread_x, last_x, near_c, last_c):
+            for copy in service(slot):
+                copy.wait_send()
+    for step in range(reps - 1):
+        for buffer, kind, part in ((all_x, 0, x_part(chip, core)), (all_c, 8, c_part(half, core))):
+            for _, _, passes, onward in hops(buffer, kind, part, step):
+                pl.when(passes)(onward.wait_send)
+
+
+def fused(reps, chips, across, inputs, cotangent, w_gate, w_upward, w_down):
+    rows, width = inputs.shape
+    hidden = w_gate.shape[1]
+    cols = width // reps
+    kind = inputs.dtype
+    piece = (rows // (2 * chips), width)
+    vmem = pl.BlockSpec(memory_space=pltpu.VMEM)
+    anywhere = pl.BlockSpec(memory_space=pl.ANY)
+    count = len(chunks_of(hidden, STREAM))
+    wide = jax.ShapeDtypeStruct((reps, rows, hidden), kind)
+    slim = jax.ShapeDtypeStruct((reps, rows, cols), kind)
+    total, hid, gd, ud, xc, cc = pl.pallas_call(
+        functools.partial(fused_kernel, reps, chips, across),
+        out_shape=(jax.ShapeDtypeStruct((chips, 2) + piece, kind), wide, wide, wide, slim, slim),
+        in_specs=[pl.BlockSpec(memory_space=pltpu.HBM)] * 5,
+        out_specs=(vmem,) * 6,
+        scratch_shapes=[
+            pltpu.VMEM((reps, rows, width), kind),
+            pltpu.VMEM((reps, rows, width), kind),
+            pltpu.VMEM((width, hidden), kind),
+            pltpu.VMEM((width, hidden), kind),
+            pltpu.VMEM((hidden, width), kind),
+            pltpu.VMEM((2 * rows, hidden), jnp.float32),
+            pltpu.VMEM((2 * rows, hidden), jnp.float32),
+            pltpu.VMEM((chips,) + piece, kind),
+            pltpu.VMEM((chips - 1,) + piece, kind),
+            pltpu.SemaphoreType.DMA((14, reps)),
+            pltpu.SemaphoreType.DMA((12, reps)),
+            pltpu.SemaphoreType.DMA((4, chips)),
+            pltpu.SemaphoreType.DMA((4, chips)),
+            pltpu.SemaphoreType.DMA((2,)),
+            pltpu.SemaphoreType.DMA((count, 3)),
+        ],
+        compiler_params=pltpu.CompilerParams(
+            collective_id=2, has_side_effects=True, vmem_limit_bytes=46 * 2**20 + 704 * 2**10
+        ),
+        name="gather_compute",
+    )(*(pltpu.with_memory_space_constraint(a, pltpu.HBM) for a in (inputs, cotangent, w_gate, w_upward, w_down)))
+    return total.reshape(rows, width), [a.reshape(reps * rows, -1) for a in (hid, gd, ud, xc, cc)]
+
+
+def weights_kernel(tall, wide_rows, hid, gd, ud, xc, cc, total, g_gate, g_up, g_down, g_in, stage, stage_down, sems, down_sems, in_sem):
+    whole = pltpu.make_async_copy(total, g_in, in_sem)
+    whole.start()
+    pending = [None] * stage.shape[0]
+    turn = 0
+    for delta, target in ((gd, g_gate), (ud, g_up)):
+        for at, size in chunks_of(xc.shape[1], (tall,)):
+            slot = turn % len(pending)
+            if pending[slot] is not None:
+                pending[slot].wait()
+            span = pl.ds(at, size)
+            stage[slot, :size] = contract_rows(xc[:, span], delta[...])
+            pending[slot] = pltpu.make_async_copy(stage.at[slot, pl.ds(0, size)], target.at[span], sems.at[slot])
+            pending[slot].start()
+            turn += 1
+    later = [None] * stage_down.shape[0]
+    turn = 0
+    for at, size in chunks_of(hid.shape[1], (wide_rows,)):
+        slot = turn % len(later)
+        if later[slot] is not None:
+            later[slot].wait()
+        span = pl.ds(at, size)
+        stage_down[slot, :size] = contract_rows(hid[:, span], cc[...])
+        later[slot] = pltpu.make_async_copy(stage_down.at[slot, pl.ds(0, size)], g_down.at[span], down_sems.at[slot])
+        later[slot].start()
+        turn += 1
+    for copy in pending + later:
+        if copy is not None:
+            copy.wait()
+    whole.wait()
+
+
+def weight_gradients(total, hid, gd, ud, xc, cc):
+    hidden, cols = hid.shape[1], xc.shape[1]
+    vmem = pl.BlockSpec(memory_space=pltpu.VMEM)
+    anywhere = pl.BlockSpec(memory_space=pl.ANY)
+    up = jax.ShapeDtypeStruct((cols, hidden), jnp.float32)
+    down = jax.ShapeDtypeStruct((hidden, cols), jnp.float32)
+    tall, wide_rows, slots = 256, 384, 3
+    return pl.pallas_call(
+        functools.partial(weights_kernel, tall, wide_rows),
+        out_shape=(up, up, down, jax.ShapeDtypeStruct(total.shape, total.dtype)),
+        in_specs=[vmem] * 6,
+        out_specs=(anywhere,) * 4,
+        scratch_shapes=[
+            pltpu.VMEM((slots, tall, hidden), jnp.float32),
+            pltpu.VMEM((slots, wide_rows, cols), jnp.float32),
+            pltpu.SemaphoreType.DMA((slots,)),
+            pltpu.SemaphoreType.DMA((slots,)),
+            pltpu.SemaphoreType.DMA,
+        ],
+        compiler_params=pltpu.CompilerParams(vmem_limit_bytes=20 * 2**20),
+        name="weight_gradients",
+    )(hid, gd, ud, xc, cc, total)
+
+
+def fits(reps, chips, across, inputs, w_gate):
+    rows, width = inputs.shape
+    hidden = w_gate.shape[1]
+    size = inputs.dtype.itemsize
+    need = size * (3 * width * hidden + 2 * reps * rows * width + 3 * reps * rows * hidden)
+    aligned = hidden % 128 == 0 and width % (128 * reps) == 0 and rows % 128 == 0
+    return aligned and chips == 4 and across == 2 and reps == 4 and need < 52 * 2**20
+
+
 def local(reps, chips, across, inputs, cotangent, w_gate, w_upward, w_down):
     rows, width = inputs.shape
+    if fits(reps, chips, across, inputs, w_gate):
+        total, parts = fused(reps, chips, across, inputs, cotangent, w_gate, w_upward, w_down)
+        grad_gate, grad_upward, grad_down, grad_input = weight_gradients(total, *parts)
+        return (grad_input, grad_gate, grad_upward, grad_down)
     all_inputs, all_cotangent = gather(reps, inputs, cotangent)
 
     gate_pre = jnp.dot(all_inputs, w_gate, preferred_element_type=jnp.float32)

time: 142 us -> 65.3 us (0.46)
  matrix products: 65.1 us -> 0 us
  Pallas kernels: 75.4 us -> 64.3 us
    dot_general x8 -> x0, matrix products: 65.1 us -> none  [the longest x3 26.8 us: contract_cols(): lax.dot_general(left, right, (((1,), (1,)), ((), ())), preferred_element_...]
    pallas_call x2, Pallas kernels: 75.4 us -> 64.3 us  [the longest x1 56.3 us: fused(): pl.pallas_call(functools.partial(fused_kernel, reps, chips, across), out_...]
where the time goes in v2:
time: 65.3 us; the launch traced here: 65.1 us
  Pallas kernels  64.3 us (98%)
  between operations  0.82 us (1%)
    pallas_call x1, Pallas kernels, fused(): pl.pallas_call(functools.partial(fused_kernel, reps, chips, across), out_...  56.3 us
    pallas_call x1, Pallas kernels, weight_gradients(): pl.pallas_call(functools.partial(weights_kernel, tall, wide_rows), out_sh...  8.02 us

profile of v2, /device:TPU:0, one launch (start us, length us, event | category | flops | bytes accessed | tf_op | source)
XLA Modules:
  0.0 65.1 jit_solution(17294038054863189329)
XLA Ops:
  0.6 56.3 %gather_compute.1 = (bf16[4,2,16,4096]{3,2,1,0:T(8,128)(2,1)S(1)}, bf16[4,128,1408]{2,1,0:T(8,128)(2,1)S(1)}, bf16[4,128,1408]{2,1,0:T(8,128)(2,1)S(1)}, bf16[4,...) custom-call(bf16[128,4096]{1,0:T(8,128)(2,1)} %x_hbm.1, ...), custom_call_target="tpu_custom_call" | custom-call | tf_op jit(solution)/shard_map/gather_compute/pallas_call | solution.py:556
  56.9 8.0 %weight_gradients.1 = (f32[1024,1408]{1,0:T(8,128)}, f32[1024,1408]{1,0:T(8,128)}, f32[1408,1024]{1,0:T(8,128)}, bf16[128,4096]{1,0:T(8,128)(2,1)}) custom-call(bf16[512,1408]{1,0:T(8,128)(2,1)S(1)} %bitcast.6, bf16[512,1408]{1,0:T(8,128)(2,1)S(1)} %bitcast.7, bf16[512,1408]{1,0:T(8,128)(2,1)S(1)} %bitcast.8, bf16[512,1024]{1,0:T(8,128)(2,1)S(1)} %bitcast.10, ...), custom_call_target="tpu_custom_call" | custom-call | tf_op jit(solution)/shard_map/weight_gradients/pallas_call | solution.py:625

commit v3 on v2

--- a/solution.py
+++ b/solution.py
@@ -435,12 +435,8 @@
             there = peer(ahead)[0]
             pair = term(there, core)[...].astype(jnp.float32) + got[there].astype(jnp.float32)
             pair_sum(ahead)[...] = pair.astype(got.dtype)
-        for ahead, copy in enumerate(spread(), 1):
-            pl.when(peer(ahead)[0] != far_chip)(copy.start)
-
-    def diagonal():
-        for ahead, copy in enumerate(spread(), 1):
-            pl.when(peer(ahead)[0] == far_chip)(copy.start)
+        for copy in spread():
+            copy.start()
 
     def reduce_second():
         total = term(chip, core)[...].astype(jnp.float32) + got[chip].astype(jnp.float32)
@@ -473,10 +469,11 @@
         (3, 0): ((hop, 0, 2), (serve, near_x, 3)),
         (3, 2): ((serve, last_x, 2),),
         (4, 0): ((serve, last_c, 2),),
-        (4, 1): ((serve, spread_x, 3), (diagonal,)),
+        (4, 1): ((serve, spread_x, 3),),
         (4, 2): ((hop, 1, 2), (serve, near_c, 3)),
-        (5, 2): ((serve, last_x, 3),),
-        (6, 1): ((serve, last_c, 3), (reduce_second,)),
+        (5, 2): ((serve, last_x, 3), (reduce_second,)),
+        (6, 1): ((serve, last_c, 3),),
+        (7, 1): ((reduce_third,),),
     }
 
     def at_slot(phase, n):
@@ -524,7 +521,7 @@
     complete_c(3)
     for n, (at, size) in enumerate(blocks):
         deltas(2, 2, at, size)
-    reduce_third()
+        at_slot(7, n)
     for copy in relays():
         copy.wait_recv()
     for condition, copy in first_sends():
@@ -588,13 +585,14 @@
     whole.start()
     pending = [None] * stage.shape[0]
     turn = 0
-    for delta, target in ((gd, g_gate), (ud, g_up)):
-        for at, size in chunks_of(xc.shape[1], (tall,)):
+    for at, size in chunks_of(xc.shape[1], (tall,)):
+        turned = xc[:, pl.ds(at, size)].T
+        for delta, target in ((gd, g_gate), (ud, g_up)):
             slot = turn % len(pending)
             if pending[slot] is not None:
                 pending[slot].wait()
             span = pl.ds(at, size)
-            stage[slot, :size] = contract_rows(xc[:, span], delta[...])
+            stage[slot, :size] = jnp.dot(turned, delta[...], preferred_element_type=jnp.float32)
             pending[slot] = pltpu.make_async_copy(stage.at[slot, pl.ds(0, size)], target.at[span], sems.at[slot])
             pending[slot].start()
             turn += 1

time: 65.3 us -> 60.8 us (0.931)
  Pallas kernels: 64.3 us -> 59.8 us
    pallas_call x1, Pallas kernels: 56.3 us -> 52 us  [fused(): pl.pallas_call(functools.partial(fused_kernel, reps, chips, across), out_...]
where the time goes in v3:
time: 60.8 us; the launch traced here: 60.7 us
  Pallas kernels  59.8 us (98%)
  between operations  0.82 us (1%)
    pallas_call x1, Pallas kernels, fused(): pl.pallas_call(functools.partial(fused_kernel, reps, chips, across), out_...  52 us
    pallas_call x1, Pallas kernels, weight_gradients(): pl.pallas_call(functools.partial(weights_kernel, tall, wide_rows), out_sh...  7.88 us

profile of v3, /device:TPU:0, one launch (start us, length us, event | category | flops | bytes accessed | tf_op | source)
XLA Modules:
  0.0 60.7 jit_solution(5414270864325052801)
XLA Ops:
  0.6 52.0 %gather_compute.1 = (bf16[4,2,16,4096]{3,2,1,0:T(8,128)(2,1)S(1)}, bf16[4,128,1408]{2,1,0:T(8,128)(2,1)S(1)}, bf16[4,128,1408]{2,1,0:T(8,128)(2,1)S(1)}, bf16[4,...) custom-call(bf16[128,4096]{1,0:T(8,128)(2,1)} %x_hbm.1, ...), custom_call_target="tpu_custom_call" | custom-call | tf_op jit(solution)/shard_map/gather_compute/pallas_call | solution.py:553
  52.6 7.9 %weight_gradients.1 = (f32[1024,1408]{1,0:T(8,128)}, f32[1024,1408]{1,0:T(8,128)}, f32[1408,1024]{1,0:T(8,128)}, bf16[128,4096]{1,0:T(8,128)(2,1)}) custom-call(bf16[512,1408]{1,0:T(8,128)(2,1)S(1)} %bitcast.6, bf16[512,1408]{1,0:T(8,128)(2,1)S(1)} %bitcast.7, bf16[512,1408]{1,0:T(8,128)(2,1)S(1)} %bitcast.8, bf16[512,1024]{1,0:T(8,128)(2,1)S(1)} %bitcast.10, ...), custom_call_target="tpu_custom_call" | custom-call | tf_op jit(solution)/shard_map/weight_gradients/pallas_call | solution.py:623
